TPU v7x, 32 devices: a whole 2x2x4 slice. The times are simulated.
32 devices in a mesh: ep: 4 (over z), tp: 8 (over y, x, core).
Axes of the slice: x: 2, y: 2, z: 4, core: 2. Of those that a mesh axis runs over, the one named last changes fastest.
Arguments:
- hidden_in: bfloat16 [48, 2048], P('ep', 'tp'), may hold values from -12 to 12
- state: float32 [48, 32, 128, 128], P('ep', 'tp'), may hold values from -3 to 3
- lower_bound: float32 [32, 128], P('tp'), may hold values from 0.05 to 0.95
- w_forget: bfloat16 [2048, 4096], P(None, 'tp'), may hold values from -0.125 to 0.125
- w_input: bfloat16 [2048, 4096], P(None, 'tp'), may hold values from -0.125 to 0.125
- w_query: bfloat16 [2048, 4096], P(None, 'tp'), may hold values from -0.125 to 0.125
- w_outgate: bfloat16 [2048, 4096], P(None, 'tp'), may hold values from -0.125 to 0.125
- head_gain: float32 [128], replicated, may hold values from 0.1 to 1.9
- w_out: bfloat16 [4096, 2048], P('tp'), may hold values from -0.125 to 0.125
- ln1_gain: float32 [2048], replicated, may hold values from 0.1 to 8
- ln1_bias: float32 [2048], replicated, may hold values from -1.5 to 1.5
- routes: int32 [48, 4], P('ep'), may hold values from 0 to 7, all different within a row; in each aligned block of 12 rows (0 to 11, 12 to 23, ...) at most 9 rows name the same one
- route_weights: float32 [48, 4], P('ep'), may hold values from 0.2 to 1.5
- exp_gate: bfloat16 [8, 2048, 4096], P('ep', None, 'tp'), may hold values from -0.125 to 0.125
- exp_up: bfloat16 [8, 2048, 4096], P('ep', None, 'tp'), may hold values from -0.125 to 0.125
- exp_down: bfloat16 [8, 4096, 2048], P('ep', 'tp'), may hold values from -0.125 to 0.125
- sh_gate: bfloat16 [2048, 512], P(None, 'tp'), may hold values from -0.125 to 0.125
- sh_up: bfloat16 [2048, 512], P(None, 'tp'), may hold values from -0.125 to 0.125
- sh_down: bfloat16 [512, 2048], P('tp'), may hold values from -0.25 to 0.25
- ln2_gain: float32 [2048], replicated, may hold values from 0.1 to 1.9
- ln2_bias: float32 [2048], replicated, may hold values from -1.5 to 1.5
Outputs:
- mixed_out: bfloat16 [48, 2048], P('ep', 'tp')
- new_state: float32 [48, 32, 128, 128], P('ep', 'tp')
Inputs may be any that keep to these rules, and one draw needn't show every extreme that they name: `routes`: each row names 4 different experts; among the rows of one index of ep (12 rows) no expert is named more than 9 times, a bound that some block reaches.
All inputs are finite; a program needn't handle non-finite values.
Results may differ from a plain program's by a relative error of at most 0.023.
Values may be sent and summed in bfloat16 or wider, within the bound.
A program may use at most 64 MiB of HBM per device.

v0:
```python
import jax
import jax.numpy as jnp
from jax import lax
from jax.sharding import PartitionSpec as P

EPS = 1e-05
ALPHA = 2.0**0.25


def rounded(value):
    return lax.optimization_barrier(value.astype(jnp.bfloat16)).astype(jnp.float32)


def local(
    hidden_in,
    state,
    lower_bound,
    w_forget,
    w_input,
    w_query,
    w_outgate,
    head_gain,
    w_out,
    ln1_gain,
    ln1_bias,
    routes,
    route_weights,
    exp_gate,
    exp_up,
    exp_down,
    sh_gate,
    sh_up,
    sh_down,
    ln2_gain,
    ln2_bias,
):
    n_tp = lax.axis_size("tp")
    n_ep = lax.axis_size("ep")
    seq_count = hidden_in.shape[0]
    col_count = hidden_in.shape[1]
    model_width = col_count * n_tp
    col_start = lax.axis_index("tp") * col_count
    heads_dev = state.shape[1]
    head_size = state.shape[2]
    top_count = routes.shape[1]
    local_experts = exp_gate.shape[0]
    expert_count = local_experts * n_ep
    capacity = max(2, 3 * seq_count * top_count // (2 * expert_count))
    slot_count = expert_count * capacity
    rows_full = lax.all_gather(hidden_in, "tp", axis=1, tiled=True)

    def project(weight):
        product = jnp.dot(rows_full, weight, preferred_element_type=jnp.float32)
        return rounded(product).reshape(seq_count, heads_dev, head_size)

    forget_pre = project(w_forget)
    forget = lower_bound + (1.0 - lower_bound) * jax.nn.sigmoid(forget_pre)
    key_part = (1.0 - lower_bound) * jax.nn.sigmoid(-forget_pre)
    values = project(w_input)
    queries = jax.nn.silu(project(w_query))
    out_gate = jax.nn.silu(project(w_outgate))
    new_state = forget[..., None] * state + key_part[..., None] * values[:, :, None, :]
    readout = jnp.einsum("bhd,bhdv->bhv", queries, new_state, precision=lax.Precision.HIGHEST)
    normed = readout * lax.rsqrt(jnp.mean(readout * readout, -1, keepdims=True) + EPS) * head_gain
    mixed = (normed * out_gate).astype(jnp.bfloat16).reshape(seq_count, heads_dev * head_size)
    branch = jnp.dot(mixed, w_out, preferred_element_type=jnp.float32)
    summed = lax.psum(branch.astype(jnp.bfloat16), "tp").astype(jnp.float32)
    residual = ALPHA * rows_full.astype(jnp.float32) + summed
    average = jnp.mean(residual, -1, keepdims=True)
    centered = residual - average
    variance = jnp.mean(centered * centered, -1, keepdims=True)
    normed_rows = (centered * lax.rsqrt(variance + EPS) * ln1_gain + ln1_bias).astype(jnp.bfloat16)
    routes_flat = routes.reshape(-1)
    one_hot = (routes_flat[:, None] == jnp.arange(expert_count, dtype=jnp.int32)[None, :]).astype(
        jnp.int32
    )
    position = jnp.sum((jnp.cumsum(one_hot, 0) - one_hot) * one_hot, 1)
    slot_index = routes_flat * capacity + position
    placing = (slot_index[:, None] == jnp.arange(slot_count, dtype=jnp.int32)[None, :]).astype(
        jnp.float32
    )
    chooser = jnp.sum(placing.reshape(seq_count, top_count, slot_count), 1).astype(jnp.bfloat16)
    weighted = jnp.sum(
        (placing * route_weights.reshape(-1)[:, None]).reshape(seq_count, top_count, slot_count), 1
    )
    own_cols = lax.dynamic_slice_in_dim(normed_rows, col_start, col_count, 1)
    picked = lax.dot_general(
        chooser, normed_rows, (((0,), (0,)), ((), ())), preferred_element_type=jnp.float32
    )
    arrived = lax.all_to_all(
        picked.astype(jnp.bfloat16).reshape(n_ep, local_experts * capacity, normed_rows.shape[1]),
        "ep",
        split_axis=0,
        concat_axis=0,
        tiled=True,
    )
    blocks = arrived.reshape(n_ep, local_experts, capacity, model_width)
    gate_part = jnp.einsum("gecd,edf->gecf", blocks, exp_gate, preferred_element_type=jnp.float32)
    up_part = jnp.einsum("gecd,edf->gecf", blocks, exp_up, preferred_element_type=jnp.float32)
    hidden_part = (jax.nn.silu(gate_part) * up_part).astype(jnp.bfloat16)
    expert_part = jnp.einsum(
        "gecf,efd->gecd", hidden_part, exp_down, preferred_element_type=jnp.float32
    )
    expert_part = expert_part.reshape(n_ep, local_experts * capacity, model_width).astype(
        jnp.bfloat16
    )
    shared_hidden = (
        jax.nn.silu(jnp.dot(normed_rows, sh_gate, preferred_element_type=jnp.float32))
        * jnp.dot(normed_rows, sh_up, preferred_element_type=jnp.float32)
    ).astype(jnp.bfloat16)
    shared_part = jnp.dot(shared_hidden, sh_down, preferred_element_type=jnp.float32)
    returned = lax.all_to_all(expert_part, "ep", split_axis=0, concat_axis=0, tiled=True)
    routed_partial = jnp.dot(
        weighted,
        returned.reshape(slot_count, model_width).astype(jnp.float32),
        precision=lax.Precision.HIGHEST,
    )
    combined = lax.psum_scatter(
        (routed_partial + shared_part).astype(jnp.bfloat16), "tp", scatter_dimension=1, tiled=True
    ).astype(jnp.float32)
    final_in = ALPHA * own_cols.astype(jnp.float32) + combined
    moments_two = lax.psum((jnp.sum(final_in, -1), jnp.sum(final_in * final_in, -1)), "tp")
    average_two = moments_two[0][:, None] / model_width
    variance_two = moments_two[1][:, None] / model_width - average_two * average_two
    gain_two = lax.dynamic_slice_in_dim(ln2_gain, col_start, col_count)
    bias_two = lax.dynamic_slice_in_dim(ln2_bias, col_start, col_count)
    mixed_out = (
        (final_in - average_two) * lax.rsqrt(variance_two + EPS) * gain_two + bias_two
    ).astype(jnp.bfloat16)
    return (mixed_out, new_state)


def solution(mesh):
    placed = (
        P("ep", "tp"),
        P("ep", "tp", None, None),
        P("tp", None),
        P(None, "tp"),
        P(None, "tp"),
        P(None, "tp"),
        P(None, "tp"),
        P(),
        P("tp", None),
        P(),
        P(),
        P("ep", None),
        P("ep", None),
        P("ep", None, "tp"),
        P("ep", None, "tp"),
        P("ep", "tp", None),
        P(None, "tp"),
        P(None, "tp"),
        P("tp", None),
        P(),
        P(),
    )
    return jax.shard_map(
        local,
        mesh=mesh,
        in_specs=placed,
        out_specs=(P("ep", "tp"), P("ep", "tp", None, None)),
        check_vma=False,
    )
```

profile of v0, /device:TPU:0, one launch (start us, length us, event | category | flops | bytes accessed | tf_op | source)
XLA Modules:
  0.0 155.0 jit_solution(1456552702936218920)
XLA Ops:
  7.2 0.9 copy.41
  8.3 0.2 select_reduce_fusion.1
  8.6 0.8 copy.43
  9.4 10.7 %all_gather.3 = bf16[12,2048]{1,0:T(8,128)(2,1)S(1)} all-gather(bf16[12,256]{1,0:T(8,128)(2,1)} %param.21), channel_id=1, replica_groups=mesh['ep'=4,'tp'=8] {'tp'}, dimensions={1}, use_global_device_ids=true | all-gather | bytes 55296 | tf_op jit(solution)/shard_map/all_gather | solution.py:50
  20.1 2.0 %convolution_convert_fusion.2 = bf16[12,512]{1,0:T(8,128)(2,1)S(1)} fusion(bf16[12,2048]{1,0:T(8,128)(2,1)S(1)} %all_gather.3, bf16[2048,512]{1,0:T(8,128)(2,1)} %param.27), kind=kOutput, calls=%fused_computation.17 | convolution fusion | flops 25171968 | bytes 2158592 | tf_op jit(solution)/shard_map/dot_general | solution.py:53
  22.1 2.0 %convolution_convert_fusion.5 = bf16[12,512]{1,0:T(8,128)(2,1)S(1)} fusion(bf16[12,2048]{1,0:T(8,128)(2,1)S(1)} %all_gather.3, bf16[2048,512]{1,0:T(8,128)(2,1)} %param.26), kind=kOutput, calls=%fused_computation.20 | convolution fusion | flops 25171968 | bytes 2158592 | tf_op jit(solution)/shard_map/dot_general | solution.py:53
  24.1 2.0 %convolution_convert_fusion.3 = bf16[12,512]{1,0:T(8,128)(2,1)S(1)} fusion(bf16[12,2048]{1,0:T(8,128)(2,1)S(1)} %all_gather.3, bf16[2048,512]{1,0:T(8,128)(2,1)} %param.25), kind=kOutput, calls=%fused_computation.18 | convolution fusion | flops 25171968 | bytes 2158592 | tf_op jit(solution)/shard_map/dot_general | solution.py:53
  26.1 2.0 %convolution_convert_fusion.4 = bf16[12,512]{1,0:T(8,128)(2,1)S(1)} fusion(bf16[12,2048]{1,0:T(8,128)(2,1)S(1)} %all_gather.3, bf16[2048,512]{1,0:T(8,128)(2,1)} %param.24), kind=kOutput, calls=%fused_computation.19 | convolution fusion | flops 25171968 | bytes 2158592 | tf_op jit(solution)/shard_map/dot_general | solution.py:53
  28.3 3.8 %multiply_add_fusion = f32[12,4,128,128]{3,2,1,0:T(8,128)S(1)} fusion(f32[12,4,128,128]{3,2,1,0:T(8,128)} %param.22, f32[12,4,128]{2,1,0:T(4,128)S(1)} %reshape.140, f32[12,4,128]{2,1,0:T(4,128)S(1)} %bitcast.85, f32[12,4,128]{2,1,0:T(4,128)S(1)} %bitcast.84), kind=kLoop, calls=%fused_computation.6 | loop fusion | flops 2359296 | bytes 6365184 | tf_op jit(solution)/shard_map/add | solution.py:62
  32.1 1.6 %copy-done.1 = f32[12,4,128,128]{3,2,1,0:T(8,128)} copy-done((f32[12,4,128,128]{3,2,1,0:T(8,128)}, f32[12,4,128,128]{3,2,1,0:T(8,128)S(1)}, u32[]{:S(2)}) %copy-start.1) | copy-done | bytes 3145752
  33.7 2.8 %fusion.51 = f32[12,4,1,128]{3,2,1,0:T(1,128)S(1)} fusion(f32[12,4,128,1]{2,3,1,0:T(1,128)S(1)} %bitcast.83, f32[12,4,128,128]{3,2,1,0:T(8,128)S(1)} %multiply_add_fusion), kind=kOutput, calls=%fused_computation.69 | convolution fusion | flops 9437184 | bytes 3194880 | tf_op jit(solution)/shard_map/bhd,bhdv->bhv/dot_general | solution.py:63
  36.7 0.4 convolution_convert_fusion.1
  37.1 23.9 %psum.21 = bf16[12,2048]{1,0:T(8,128)(2,1)S(1)} all-reduce(bf16[12,2048]{1,0:T(8,128)(2,1)S(1)} %convolution_convert_fusion.1), channel_id=1, replica_groups=mesh['ep'=4,'tp'=8] {'tp'}, use_global_device_ids=true, to_apply=%region_1.2 | all-reduce | flops 24576 | bytes 98304 | tf_op jit(solution)/shard_map/psum | solution.py:67
  61.1 0.2 multiply_reduce_fusion
  61.6 0.3 convolution_convert_fusion
  62.0 13.9 %all_to_all.10 = bf16[4,18,2048]{2,1,0:T(8,128)(2,1)S(1)} all-to-all(bf16[4,18,2048]{2,1,0:T(8,128)(2,1)S(1)} %reshape.135), channel_id=1, replica_groups=mesh['ep'=4,'tp'=8] {'ep'}, dimensions={0} | all-to-all | bytes 589824 | tf_op jit(solution)/shard_map/all_to_all | solution.py:90
  75.8 0.2 copy.44
  76.0 2.9 %fusion.13 = f32[4,2,9,512]{3,2,0,1:T(8,128)S(1)} fusion(bf16[2,2048,512]{2,1,0:T(8,128)(2,1)} %param.34, bf16[4,2,9,2048]{3,0,2,1:T(4,128)(2,1)S(1)} %bitcast.78), kind=kOutput, calls=%fused_computation.13 | convolution fusion | flops 150994944 | bytes 4636672 | tf_op jit(solution)/shard_map/gecd,edf->gecf/dot_general | solution.py:98
  79.0 5.0 %fusion.9 = bf16[4,2,9,2048]{3,2,0,1:T(8,128)(2,1)S(1)} fusion(bf16[2,512,2048]{2,1,0:T(8,128)(2,1)} %param.36, bf16[2,2048,512]{2,1,0:T(8,128)(2,1)} %param.35, bf16[4,2,9,2048]{3,0,2,1:T(4,128)(2,1)S(1)} %bitcast.79, f32[4,2,9,512]{3,2,0,1:T(8,128)S(1)} %fusion.13), kind=kOutput, calls=%fused_computation.8 | convolution fusion | flops 302358528 | bytes 9125888 | tf_op jit(solution)/shard_map/gecf,efd->gecd/dot_general | solution.py:101
  84.0 0.2 copy.47
  84.2 0.9 copy.48
  85.2 3.5 %all-to-all-start.1 = ((bf16[4,18,2048]{2,1,0:T(8,128)(2,1)}), bf16[4,18,2048]{2,1,0:T(8,128)(2,1)S(1)}, u32[]{:S(2)}, u32[]{:S(2)}) async-start(bf16[4,18,2048]{2,1,0:T(8,128)(2,1)} %copy.48), calls=%async_computation.1 | async-start | bytes 786432 | tf_op jit(solution)/shard_map/all_to_all | solution.py:112
  88.7 1.1 fusion.53
  89.8 8.4 %all-to-all-done.1 = bf16[4,18,2048]{2,1,0:T(8,128)(2,1)S(1)} async-done(((bf16[4,18,2048]{2,1,0:T(8,128)(2,1)}), bf16[4,18,2048]{2,1,0:T(8,128)(2,1)S(1)}, u32[]{:S(2)}, u32[]{:S(2)}) %all-to-all-start.1) | async-done | bytes 294944 | tf_op jit(solution)/shard_map/all_to_all | solution.py:112
  98.2 0.3 fusion.52
  98.5 2.0 %fusion.12 = bf16[12,2048]{1,0:T(8,128)(2,1)} fusion(f32[12,2048]{1,0:T(8,128)S(1)} %fusion.52, bf16[64,2048]{1,0:T(8,128)(2,1)S(1)} %copy-done.2, bf16[12,2048]{1,0:T(8,128)(2,1)S(1)} %add_convert_fusion, bf16[2048,64]{0,1:T(8,128)(2,1)} %param.38, f32[12,64]{1,0:T(8,128)S(1)} %fusion.53), kind=kOutput, calls=%fused_computation.11 | convolution fusion | flops 6345216 | bytes 723968 | tf_op jit(solution)/shard_map/dot_general | solution.py:111
  100.5 0.8 dynamic_slice.11
  101.3 0.8 dynamic_slice.10
  102.0 31.7 %reduce-scatter.2.cloned.1.call-done = bf16[12,256]{1,0:T(8,128)(2,1)} async-done(((bf16[12,2048]{1,0:T(8,128)(2,1)}), bf16[12,256]{1,0:T(8,128)(2,1)}) %reduce-scatter.2.cloned.1.call-update) | async-done | bytes 6160 | tf_op jit(solution)/shard_map/reduce_scatter | solution.py:118
  133.8 0.8 fusion.41
  134.6 12.2 %all-reduce = (f32[12]{0:T(128)S(1)}, f32[12]{0:T(128)S(1)}) all-reduce(f32[12]{0:T(128)S(1)} %get-tuple-element.3, f32[12]{0:T(128)S(1)} %get-tuple-element.2), channel_id=1, replica_groups=mesh['ep'=4,'tp'=8] {'tp'}, use_global_device_ids=true, to_apply=%region_12.13 | all-reduce | flops 24 | bytes 192 | tf_op jit(solution)/shard_map/psum | solution.py:122
  146.8 1.4 add_convert_fusion.1
  (44 shorter events, 1.4 us)
Async XLA Ops:
  7.2 29.6 %copy-start = (bf16[512,2048]{1,0:T(8,128)(2,1)S(1)}, bf16[512,2048]{1,0:T(8,128)(2,1)}, u32[]{:S(2)}) copy-start(bf16[512,2048]{1,0:T(8,128)(2,1)} %param.29) | copy-start | bytes 6291460
  22.1 6.1 %copy-start.3 = (f32[4,128]{1,0:T(4,128)S(1)}, f32[4,128]{1,0:T(4,128)}, u32[]{:S(2)}) copy-start(f32[4,128]{1,0:T(4,128)} %param.23) | copy-start | bytes 6148
  32.1 1.7 %copy-start.1 = (f32[12,4,128,128]{3,2,1,0:T(8,128)}, f32[12,4,128,128]{3,2,1,0:T(8,128)S(1)}, u32[]{:S(2)}) copy-start(f32[12,4,128,128]{3,2,1,0:T(8,128)S(1)} %multiply_add_fusion) | copy-start | bytes 9437188
  32.1 4.5 %copy-start.6 = (f32[128]{0:T(128)S(1)}, f32[128]{0:T(128)}, u32[]{:S(2)}) copy-start(f32[128]{0:T(128)} %param.28) | copy-start | bytes 1540
  32.1 29.4 %copy-start.4 = (f32[2048]{0:T(1024)S(1)}, f32[2048]{0:T(1024)}, u32[]{:S(2)}) copy-start(f32[2048]{0:T(1024)} %param.31) | copy-start | bytes 24580
  32.1 29.4 %copy-start.5 = (f32[2048]{0:T(1024)S(1)}, f32[2048]{0:T(1024)}, u32[]{:S(2)}) copy-start(f32[2048]{0:T(1024)} %param.30) | copy-start | bytes 24580
  84.0 14.5 %copy-start.2 = (bf16[64,2048]{1,0:T(8,128)(2,1)S(1)}, bf16[64,2048]{1,0:T(8,128)(2,1)}, u32[]{:S(2)}) copy-start(bf16[64,2048]{1,0:T(8,128)(2,1)} %param.39) | copy-start | bytes 786436
  85.2 13.0 %all-to-all-start.1 = ((bf16[4,18,2048]{2,1,0:T(8,128)(2,1)}), bf16[4,18,2048]{2,1,0:T(8,128)(2,1)S(1)}, u32[]{:S(2)}, u32[]{:S(2)}) async-start(bf16[4,18,2048]{2,1,0:T(8,128)(2,1)} %copy.48), calls=%async_computation.1 | async-start | bytes 786432 | tf_op jit(solution)/shard_map/all_to_all | solution.py:112
  88.6 45.2 %reduce-scatter.2.cloned.1.call-start = ((), (), s32[]{:S(2)}) async-start(), calls=%async_computation.3 | async-start | bytes 73728 | tf_op jit(solution)/shard_map/reduce_scatter | solution.py:118
Sparse Core Ops, SparseCore 0:
  100.6 33.1 reduce-scatter.1
where the time goes:
time: 156 us; the launch traced here: 155 us
  blocking collectives  60.6 us (39%)
  waiting for transfers between devices  40.1 us (26%)
  matrix products  22.5 us (14%)
  between operations  14.3 us (9%)
  other arithmetic  7.16 us (5%)
  local copies, waits for them, and re-layouts  6.75 us (4%)
  starting transfers between devices  3.5 us (2%)
    reduce_scatter x1, waiting for transfers between devices, local(): lax.psum_scatter((routed_partial + shared_part).astype(jnp.bfloat16), 'tp...  31.7 us
    psum x1, blocking collectives, local(): summed = lax.psum(branch.astype(jnp.bfloat16), 'tp').astype(jnp.float32)  23.9 us
    all_to_all x1, blocking collectives, local(): lax.all_to_all(picked.astype(jnp.bfloat16).reshape(n_ep, local_experts *...  13.9 us
    psum x1, blocking collectives, local(): lax.psum((jnp.sum(final_in, -1), jnp.sum(final_in * final_in, -1)), 'tp')  12.2 us
    all_gather x1, blocking collectives, local(): rows_full = lax.all_gather(hidden_in, 'tp', axis=1, tiled=True)  10.7 us
    all_to_all x1, waiting for transfers between devices, local(): lax.all_to_all(expert_part, 'ep', split_axis=0, concat_axis=0, tiled=True)  8.36 us
    dot_general x4, matrix products, project(): product = jnp.dot(rows_full, weight, preferred_element_type=jnp.float32)  7.85 us
    dot_general x1, matrix products, local(): jnp.einsum('gecf,efd->gecd', hidden_part, exp_down, preferred_element_typ...  4.99 us
  transfers between devices with their start and end apart: 2, of which 2 were waited for; matrix products, arithmetic and copies ran while one was open for 2% of the time, Pallas kernels for 0%

commit v1 on v0

--- a/solution.py
+++ b/solution.py
@@ -47,7 +47,8 @@
     expert_count = local_experts * n_ep
     capacity = max(2, 3 * seq_count * top_count // (2 * expert_count))
     slot_count = expert_count * capacity
-    rows_full = lax.all_gather(hidden_in, "tp", axis=1, tiled=True)
+    met_up = jax.lax.all_gather(hidden_in, axis_name="tp")
+    rows_full = jnp.concatenate(met_up, axis=1)
 
     def project(weight):
         product = jnp.dot(rows_full, weight, preferred_element_type=jnp.float32)

time: 156 us -> 156 us (level)
  no operation moved by 1% of the time
where the time goes in v1:
time: 156 us; the launch traced here: 155 us
  blocking collectives  60.9 us (39%)
  waiting for transfers between devices  40.1 us (26%)
  matrix products  22.6 us (14%)
  between operations  14.3 us (9%)
  other arithmetic  7.16 us (5%)
  local copies, waits for them, and re-layouts  6.79 us (4%)
  starting transfers between devices  3.5 us (2%)
    reduce_scatter x1, waiting for transfers between devices, local(): lax.psum_scatter((routed_partial + shared_part).astype(jnp.bfloat16), 'tp...  31.7 us
    psum x1, blocking collectives, local(): summed = lax.psum(branch.astype(jnp.bfloat16), 'tp').astype(jnp.float32)  24 us
    all_to_all x1, blocking collectives, local(): lax.all_to_all(picked.astype(jnp.bfloat16).reshape(n_ep, local_experts *...  13.9 us
    psum x1, blocking collectives, local(): lax.psum((jnp.sum(final_in, -1), jnp.sum(final_in * final_in, -1)), 'tp')  12.1 us
    all_gather x1, blocking collectives, local(): met_up = jax.lax.all_gather(hidden_in, axis_name='tp')  10.9 us
    all_to_all x1, waiting for transfers between devices, local(): lax.all_to_all(expert_part, 'ep', split_axis=0, concat_axis=0, tiled=True)  8.36 us
    dot_general x4, matrix products, project(): product = jnp.dot(rows_full, weight, preferred_element_type=jnp.float32)  7.86 us
    dot_general x1, matrix products, local(): jnp.einsum('gecf,efd->gecd', hidden_part, exp_down, preferred_element_typ...  5 us
  transfers between devices with their start and end apart: 2, of which 2 were waited for; matrix products, arithmetic and copies ran while one was open for 2% of the time, Pallas kernels for 0%

profile of v1, /device:TPU:0, one launch (start us, length us, event | category | flops | bytes accessed | tf_op | source)
XLA Modules:
  0.0 155.4 jit_solution(14068929202801168686)
XLA Ops:
  7.2 0.9 copy.45
  8.3 0.2 select_reduce_fusion.1
  8.6 0.8 copy.47
  9.4 10.9 %all-gather.1 = bf16[8,12,256]{2,1,0:T(8,128)(2,1)S(1)} all-gather(bf16[1,12,256]{2,1,0:T(8,128)(2,1)} %bitcast.106), channel_id=2, replica_groups=mesh['ep'=4,'tp'=8] {'tp'}, dimensions={0}, use_global_device_ids=true | all-gather | bytes 55296 | tf_op jit(solution)/shard_map/all_gather | solution.py:50
  20.3 2.0 %convolution_convert_fusion.2 = bf16[12,512]{1,0:T(8,128)(2,1)S(1)} fusion(bf16[12,2048]{1,0:T(8,128)(2,1)S(1)} %bitcast.85, bf16[2048,512]{1,0:T(8,128)(2,1)} %param.27), kind=kOutput, calls=%fused_computation.17 | convolution fusion | flops 25171968 | bytes 2158592 | tf_op jit(solution)/shard_map/dot_general | solution.py:54
  22.3 2.0 %convolution_convert_fusion.5 = bf16[12,512]{1,0:T(8,128)(2,1)S(1)} fusion(bf16[12,2048]{1,0:T(8,128)(2,1)S(1)} %bitcast.86, bf16[2048,512]{1,0:T(8,128)(2,1)} %param.26), kind=kOutput, calls=%fused_computation.20 | convolution fusion | flops 25171968 | bytes 2158592 | tf_op jit(solution)/shard_map/dot_general | solution.py:54
  24.4 2.0 %convolution_convert_fusion.3 = bf16[12,512]{1,0:T(8,128)(2,1)S(1)} fusion(bf16[12,2048]{1,0:T(8,128)(2,1)S(1)} %bitcast.87, bf16[2048,512]{1,0:T(8,128)(2,1)} %param.25), kind=kOutput, calls=%fused_computation.18 | convolution fusion | flops 25171968 | bytes 2158592 | tf_op jit(solution)/shard_map/dot_general | solution.py:54
  26.4 2.0 %convolution_convert_fusion.4 = bf16[12,512]{1,0:T(8,128)(2,1)S(1)} fusion(bf16[12,2048]{1,0:T(8,128)(2,1)S(1)} %bitcast.88, bf16[2048,512]{1,0:T(8,128)(2,1)} %param.24), kind=kOutput, calls=%fused_computation.19 | convolution fusion | flops 25171968 | bytes 2158592 | tf_op jit(solution)/shard_map/dot_general | solution.py:54
  28.5 3.8 %multiply_add_fusion = f32[12,4,128,128]{3,2,1,0:T(8,128)S(1)} fusion(f32[12,4,128,128]{3,2,1,0:T(8,128)} %param.22, f32[12,4,128]{2,1,0:T(4,128)S(1)} %reshape.148, f32[12,4,128]{2,1,0:T(4,128)S(1)} %bitcast.99, f32[12,4,128]{2,1,0:T(4,128)S(1)} %bitcast.98), kind=kLoop, calls=%fused_computation.6 | loop fusion | flops 2359296 | bytes 6365184 | tf_op jit(solution)/shard_map/add | solution.py:63
  32.3 1.6 %copy-done.1 = f32[12,4,128,128]{3,2,1,0:T(8,128)} copy-done((f32[12,4,128,128]{3,2,1,0:T(8,128)}, f32[12,4,128,128]{3,2,1,0:T(8,128)S(1)}, u32[]{:S(2)}) %copy-start.1) | copy-done | bytes 3145752
  34.0 2.8 %fusion.51 = f32[12,4,1,128]{3,2,1,0:T(1,128)S(1)} fusion(f32[12,4,128,1]{2,3,1,0:T(1,128)S(1)} %bitcast.97, f32[12,4,128,128]{3,2,1,0:T(8,128)S(1)} %multiply_add_fusion), kind=kOutput, calls=%fused_computation.69 | convolution fusion | flops 9437184 | bytes 3194880 | tf_op jit(solution)/shard_map/bhd,bhdv->bhv/dot_general | solution.py:64
  37.0 0.4 convolution_convert_fusion.1
  37.3 24.0 %psum.21 = bf16[12,2048]{1,0:T(8,128)(2,1)S(1)} all-reduce(bf16[12,2048]{1,0:T(8,128)(2,1)S(1)} %convolution_convert_fusion.1), channel_id=1, replica_groups=mesh['ep'=4,'tp'=8] {'tp'}, use_global_device_ids=true, to_apply=%region_1.2 | all-reduce | flops 24576 | bytes 98304 | tf_op jit(solution)/shard_map/psum | solution.py:68
  61.5 0.2 multiply_reduce_fusion
  62.0 0.3 convolution_convert_fusion
  62.3 13.9 %all_to_all.10 = bf16[4,18,2048]{2,1,0:T(8,128)(2,1)S(1)} all-to-all(bf16[4,18,2048]{2,1,0:T(8,128)(2,1)S(1)} %reshape.143), channel_id=1, replica_groups=mesh['ep'=4,'tp'=8] {'ep'}, dimensions={0} | all-to-all | bytes 589824 | tf_op jit(solution)/shard_map/all_to_all | solution.py:91
  76.2 0.2 copy.48
  76.4 2.9 %fusion.13 = f32[4,2,9,512]{3,2,0,1:T(8,128)S(1)} fusion(bf16[2,2048,512]{2,1,0:T(8,128)(2,1)} %param.34, bf16[4,2,9,2048]{3,0,2,1:T(4,128)(2,1)S(1)} %bitcast.83), kind=kOutput, calls=%fused_computation.13 | convolution fusion | flops 150994944 | bytes 4636672 | tf_op jit(solution)/shard_map/gecd,edf->gecf/dot_general | solution.py:99
  79.4 5.0 %fusion.9 = bf16[4,2,9,2048]{3,2,0,1:T(8,128)(2,1)S(1)} fusion(bf16[2,512,2048]{2,1,0:T(8,128)(2,1)} %param.36, bf16[2,2048,512]{2,1,0:T(8,128)(2,1)} %param.35, bf16[4,2,9,2048]{3,0,2,1:T(4,128)(2,1)S(1)} %bitcast.84, f32[4,2,9,512]{3,2,0,1:T(8,128)S(1)} %fusion.13), kind=kOutput, calls=%fused_computation.8 | convolution fusion | flops 302358528 | bytes 9125888 | tf_op jit(solution)/shard_map/gecf,efd->gecd/dot_general | solution.py:102
  84.4 0.3 copy.51
  84.6 0.9 copy.52
  85.5 3.5 %all-to-all-start.1 = ((bf16[4,18,2048]{2,1,0:T(8,128)(2,1)}), bf16[4,18,2048]{2,1,0:T(8,128)(2,1)S(1)}, u32[]{:S(2)}, u32[]{:S(2)}) async-start(bf16[4,18,2048]{2,1,0:T(8,128)(2,1)} %copy.52), calls=%async_computation.1 | async-start | bytes 786432 | tf_op jit(solution)/shard_map/all_to_all | solution.py:113
  89.1 1.1 fusion.53
  90.2 8.4 %all-to-all-done.1 = bf16[4,18,2048]{2,1,0:T(8,128)(2,1)S(1)} async-done(((bf16[4,18,2048]{2,1,0:T(8,128)(2,1)}), bf16[4,18,2048]{2,1,0:T(8,128)(2,1)S(1)}, u32[]{:S(2)}, u32[]{:S(2)}) %all-to-all-start.1) | async-done | bytes 294944 | tf_op jit(solution)/shard_map/all_to_all | solution.py:113
  98.6 0.2 fusion.52
  98.9 2.0 %fusion.12 = bf16[12,2048]{1,0:T(8,128)(2,1)} fusion(f32[12,2048]{1,0:T(8,128)S(1)} %fusion.52, bf16[64,2048]{1,0:T(8,128)(2,1)} %param.39, bf16[12,2048]{1,0:T(8,128)(2,1)S(1)} %add_convert_fusion, bf16[2048,64]{0,1:T(8,128)(2,1)} %param.38, f32[12,64]{1,0:T(8,128)S(1)} %fusion.53), kind=kOutput, calls=%fused_computation.11 | convolution fusion | flops 6345216 | bytes 723968 | tf_op jit(solution)/shard_map/dot_general | solution.py:112
  101.0 0.8 dynamic_slice.11
  101.7 0.8 dynamic_slice.10
  102.5 31.7 %reduce-scatter.2.cloned.1.call-done = bf16[12,256]{1,0:T(8,128)(2,1)} async-done(((bf16[12,2048]{1,0:T(8,128)(2,1)}), bf16[12,256]{1,0:T(8,128)(2,1)}) %reduce-scatter.2.cloned.1.call-update) | async-done | bytes 6160 | tf_op jit(solution)/shard_map/reduce_scatter | solution.py:119
  134.2 0.8 fusion.41
  135.0 12.1 %all-reduce = (f32[12]{0:T(128)S(1)}, f32[12]{0:T(128)S(1)}) all-reduce(f32[12]{0:T(128)S(1)} %get-tuple-element.3, f32[12]{0:T(128)S(1)} %get-tuple-element.2), channel_id=1, replica_groups=mesh['ep'=4,'tp'=8] {'tp'}, use_global_device_ids=true, to_apply=%region_12.13 | all-reduce | flops 24 | bytes 192 | tf_op jit(solution)/shard_map/psum | solution.py:123
  147.2 1.4 add_convert_fusion.1
  (45 shorter events, 1.4 us)
Async XLA Ops:
  7.2 29.8 %copy-start = (bf16[512,2048]{1,0:T(8,128)(2,1)S(1)}, bf16[512,2048]{1,0:T(8,128)(2,1)}, u32[]{:S(2)}) copy-start(bf16[512,2048]{1,0:T(8,128)(2,1)} %param.29) | copy-start | bytes 6291460
  22.3 6.1 %copy-start.2 = (f32[4,128]{1,0:T(4,128)S(1)}, f32[4,128]{1,0:T(4,128)}, u32[]{:S(2)}) copy-start(f32[4,128]{1,0:T(4,128)} %param.23) | copy-start | bytes 6148
  32.3 1.7 %copy-start.1 = (f32[12,4,128,128]{3,2,1,0:T(8,128)}, f32[12,4,128,128]{3,2,1,0:T(8,128)S(1)}, u32[]{:S(2)}) copy-start(f32[12,4,128,128]{3,2,1,0:T(8,128)S(1)} %multiply_add_fusion) | copy-start | bytes 9437188
  32.3 4.5 %copy-start.5 = (f32[128]{0:T(128)S(1)}, f32[128]{0:T(128)}, u32[]{:S(2)}) copy-start(f32[128]{0:T(128)} %param.28) | copy-start | bytes 1540
  32.3 29.6 %copy-start.3 = (f32[2048]{0:T(1024)S(1)}, f32[2048]{0:T(1024)}, u32[]{:S(2)}) copy-start(f32[2048]{0:T(1024)} %param.31) | copy-start | bytes 24580
  32.3 29.6 %copy-start.4 = (f32[2048]{0:T(1024)S(1)}, f32[2048]{0:T(1024)}, u32[]{:S(2)}) copy-start(f32[2048]{0:T(1024)} %param.30) | copy-start | bytes 24580
  85.5 13.0 %all-to-all-start.1 = ((bf16[4,18,2048]{2,1,0:T(8,128)(2,1)}), bf16[4,18,2048]{2,1,0:T(8,128)(2,1)S(1)}, u32[]{:S(2)}, u32[]{:S(2)}) async-start(bf16[4,18,2048]{2,1,0:T(8,128)(2,1)} %copy.52), calls=%async_computation.1 | async-start | bytes 786432 | tf_op jit(solution)/shard_map/all_to_all | solution.py:113
  89.0 45.2 %reduce-scatter.2.cloned.1.call-start = ((), (), s32[]{:S(2)}) async-start(), calls=%async_computation.3 | async-start | bytes 73728 | tf_op jit(solution)/shard_map/reduce_scatter | solution.py:119
Sparse Core Ops, SparseCore 0:
  101.1 33.0 reduce-scatter.1
